TPU v7x, 32 devices: a whole 2x2x4 slice. The times are simulated.
32 devices in a mesh: sp: 8 (over z, y), tp: 4 (over x, core).
Axes of the slice: x: 2, y: 2, z: 4, core: 2. Of those that a mesh axis runs over, the one named last changes fastest.
Arguments:
- tokens: bfloat16 [4096, 2048], P(('sp', 'tp')), may hold values from -6 to 6
- queries: bfloat16 [4096, 1024], P('sp', 'tp'), may hold values from -160 to 160
- keys: bfloat16 [4096, 1024], P('sp', 'tp'), may hold values from -8 to 8
- values: bfloat16 [4096, 1024], P('sp', 'tp'), may hold values from -6 to 6
- lambdas: float32 [8], P('tp'), may hold values from 0.3 to 0.8
- head_gain: float32 [128], replicated, may hold values from 0.1 to 1.9
- out_weight: bfloat16 [1024, 2048], replicated, may hold values from -0.1875 to 0.1875
- mixer_gain: float32 [2048], replicated, may hold values from 0.1 to 1.9
- up_weight: bfloat16 [2048, 4096], P('sp', 'tp'), may hold values from -0.125 to 0.125
- down_weight: bfloat16 [4096, 2048], P('tp', 'sp'), may hold values from -0.09375 to 0.09375
Outputs:
- result: bfloat16 [4096, 2048], P(('sp', 'tp'))
All inputs are finite; a program needn't handle non-finite values.
Results may differ from a plain program's by a relative error of at most 0.02.
Values may be sent and summed in bfloat16 or wider, within the bound.
A program may use at most 128 MiB of HBM per device.

v0:
```python
import math
import jax
import jax.numpy as jnp
from jax import lax
from jax.sharding import PartitionSpec as P

DQK = 64
DV = 128


def per_device(
    tokens,
    queries,
    keys,
    values,
    lambdas,
    head_gain,
    out_weight,
    mixer_gain,
    up_weight,
    down_weight,
):
    tok_rows = queries.shape[0]
    head_count = lambdas.shape[0]
    scaling = DQK ** (-0.5)
    sp_index = lax.axis_index("sp")
    first_row = sp_index * tok_rows
    last_row = first_row + tok_rows - 1
    query_split = queries.reshape(tok_rows, head_count, 2, DQK)
    query_pos = first_row + lax.broadcasted_iota(jnp.int32, (tok_rows, 1), 0)
    floor_max = jnp.full((head_count, tok_rows), -1e30, jnp.float32)
    zero_total = jnp.zeros((head_count, tok_rows), jnp.float32)
    zero_acc = jnp.zeros((head_count, tok_rows, DV), jnp.float32)
    start_state = (floor_max, zero_total, zero_acc, floor_max, zero_total, zero_acc)
    key_piece = lax.all_gather(keys, "sp", axis=0, tiled=True)
    value_piece = lax.all_gather(values, "sp", axis=0, tiled=True)
    piece_rows = key_piece.shape[0]
    block_width = math.gcd(piece_rows, 512)

    def one_block(block_index, running):
        offset = block_index * block_width

        def update(inner):
            key_block = lax.dynamic_slice_in_dim(key_piece, offset, block_width, 0).reshape(
                block_width, head_count, 2, DQK
            )
            value_block = lax.dynamic_slice_in_dim(value_piece, offset, block_width, 0).reshape(
                block_width, head_count, DV
            )
            key_pos = offset + lax.broadcasted_iota(jnp.int32, (1, block_width), 1)
            allowed = key_pos <= query_pos
            updated = []
            for map_index in range(2):
                run_max = inner[3 * map_index]
                run_total = inner[3 * map_index + 1]
                run_acc = inner[3 * map_index + 2]
                scores = (
                    jnp.einsum(
                        "qhd,khd->hqk",
                        query_split[:, :, map_index],
                        key_block[:, :, map_index],
                        preferred_element_type=jnp.float32,
                    )
                    * scaling
                )
                scores = jnp.where(allowed[None], scores, -jnp.inf)
                new_max = jnp.maximum(run_max, jnp.max(scores, axis=2))
                shrink = jnp.exp(run_max - new_max)
                exponent = jnp.exp(scores - new_max[:, :, None])
                new_total = run_total * shrink + jnp.sum(exponent, axis=2)
                new_acc = run_acc * shrink[:, :, None] + jnp.einsum(
                    "hqk,khd->hqd",
                    exponent.astype(jnp.bfloat16),
                    value_block,
                    preferred_element_type=jnp.float32,
                )
                updated += [new_max, new_total, new_acc]
            return tuple(updated)

        return lax.cond(offset <= last_row, update, lambda inner: inner, running)

    final = lax.fori_loop(0, piece_rows // block_width, one_block, start_state)
    first_map = final[2] / final[1][:, :, None]
    second_map = final[5] / final[4][:, :, None]
    differ = first_map - lambdas[:, None, None] * second_map
    spread = lax.rsqrt(jnp.mean(differ * differ, axis=2, keepdims=True) + 1e-06)
    attended = (differ * spread * head_gain).astype(jnp.bfloat16)
    attended = jnp.transpose(attended, (1, 0, 2)).reshape(tok_rows, head_count * DV)
    all_heads = lax.all_to_all(attended, "tp", split_axis=0, concat_axis=1, tiled=True)
    projected = jnp.dot(all_heads, out_weight, preferred_element_type=jnp.float32).astype(
        jnp.bfloat16
    )
    resid = (tokens.astype(jnp.float32) + projected.astype(jnp.float32)).astype(jnp.bfloat16)
    resid_full = resid.astype(jnp.float32)
    normed = (
        resid_full
        * lax.rsqrt(jnp.mean(resid_full * resid_full, axis=1, keepdims=True) + 1e-06)
        * mixer_gain
    ).astype(jnp.bfloat16)
    up_full, down_full = (
        lax.all_gather(up_weight, "sp", axis=0, tiled=True),
        lax.all_gather(down_weight, "sp", axis=1, tiled=True),
    )
    hidden = jnp.square(
        jax.nn.relu(
            jnp.dot(
                lax.all_gather(normed, "tp", axis=0, tiled=True),
                up_full,
                preferred_element_type=jnp.float32,
            )
        )
    ).astype(jnp.bfloat16)
    mixed = lax.psum_scatter(
        jnp.dot(hidden, down_full, preferred_element_type=jnp.float32).astype(jnp.bfloat16),
        "tp",
        scatter_dimension=0,
        tiled=True,
    ).astype(jnp.float32)
    return (resid_full + mixed).astype(jnp.bfloat16)


def solution(mesh):
    placed = (
        P(("sp", "tp"), None),
        P("sp", "tp"),
        P("sp", "tp"),
        P("sp", "tp"),
        P("tp"),
        P(),
        P(),
        P(),
        P("sp", "tp"),
        P("tp", "sp"),
    )
    return jax.shard_map(
        per_device, mesh=mesh, in_specs=placed, out_specs=P(("sp", "tp"), None), check_vma=False
    )
```

profile of v0, /device:TPU:0, one launch (start us, length us, event | category | flops | bytes accessed | tf_op | source)
XLA Modules:
  0.0 390.4 jit_solution(7003081648482967234)
XLA Ops:
  6.5 0.0 all-gather.6.cloned.1.call-start
  6.5 1.8 copy.19
  8.3 0.0 all-gather.6.cloned.1.call-update
  8.4 0.0 all-gather.8.cloned.1.call-start
  8.4 1.8 copy.21
  10.2 0.0 all-gather.8.cloned.1.call-update
  10.2 0.0 all-gather.10.cloned.1.call-start
  10.3 1.1 copy.20
  11.4 51.1 %all-gather.6.cloned.1.call-done = bf16[4096,256]{0,1:T(8,128)(2,1)} async-done(((bf16[512,256]{0,1:T(8,128)(2,1)}), bf16[4096,256]{0,1:T(8,128)(2,1)}) %all-gather.6.cloned.1.call-update) | async-done | bytes 2097168 | tf_op jit(solution)/shard_map/all_gather | solution.py:35
  62.5 50.6 %all-gather.8.cloned.1.call-done = bf16[4096,256]{0,1:T(8,128)(2,1)} async-done(((bf16[512,256]{0,1:T(8,128)(2,1)}), bf16[4096,256]{0,1:T(8,128)(2,1)}) %all-gather.8.cloned.1.call-update) | async-done | bytes 2097168 | tf_op jit(solution)/shard_map/all_gather | solution.py:36
  113.2 0.0 copy-start.2
  113.2 0.0 copy-start.3
  113.2 6.1 %while.24 = (s32[]{:T(128)}, f32[2,512]{1,0:T(2,128)S(1)}, f32[2,512]{1,0:T(2,128)S(1)}, f32[2,512,128]{2,1,0:T(8,128)S(1)}, f32[2,512]{1,0:T(2,128)S(1)}, /*ind...) while((s32[]{:T(128)}, f32[2,512]{1,0:T(2,128)S(1)}, ...), condition=%wide.region_7.8_spmd.clone, body=%wide.region_0.7_spmd.clone.sunk | while | flops 410784768 | bytes 17707416 | solution.py:82
  113.3 5.6 %conditional.3 = ((f32[2,512]{1,0:T(2,128)S(1)}, f32[2,512]{1,0:T(2,128)S(1)}, f32[2,512,128]{2,1,0:T(8,128)S(1)}, f32[2,512]{1,0:T(2,128)S(1)}, f32[2,512]{1,0:T(2,128)S(1)}, /*index=5*/f32[2,512,128]{2,1,0:T(8,128)S(1)})) conditional(s32[]{:T(128)} %convert_element_type.94, (f32[2,512]{1,0:T(2,128)S(1)}, f32[2,512]{1,0:T(2,128)S(1)}, ...), branch_computations={%region_1.0_spmd, %region_2.6_spmd} | conditional | flops 410784768 | bytes 17705066 | solution.py:80
  113.3 1.0 constant_dynamic-slice_fusion.1
  114.3 0.2 broadcast_compare_fusion
  114.5 0.6 fusion.20
  115.2 0.3 fusion.3
  115.5 0.6 fusion.21
  116.1 0.3 fusion.5
  116.4 1.0 constant_dynamic-slice_fusion
  117.4 0.7 convolution_add_fusion
  118.1 0.7 convolution_add_fusion.1
  119.3 0.0 copy-done.2
  119.3 0.0 copy-start
  119.3 0.5 multiply_reduce_fusion.1
  119.9 0.0 copy-done.3
  119.9 0.2 fusion.18
  120.1 0.3 copy.23
  120.4 0.2 all_to_all.14
  120.5 8.5 %all_to_all.19 = bf16[4,128,256]{2,1,0:T(8,128)(2,1)S(1)} all-to-all(bf16[4,128,256]{2,1,0:T(8,128)(2,1)S(1)} %all_to_all.14), channel_id=1, replica_groups=mesh['sp'=8,'tp'=4] {'tp'}, dimensions={0} | all-to-all | bytes 524288 | tf_op jit(solution)/shard_map/all_to_all | solution.py:89
  129.1 0.2 copy.24
  129.3 0.0 copy-done
  129.3 0.0 copy-start.1
  129.3 3.0 multiply_reduce_fusion
  132.3 0.0 copy-done.1
  132.3 1.0 multiply_convert_fusion.1
  133.3 0.0 all-gather.10.cloned.1.call-update
  133.3 0.0 all-gather.12.cloned.1.call-start
  133.3 0.5 all-gather.12.cloned.1.call-update
  133.9 0.0 all-gather.14.cloned.1.call-start
  133.9 0.5 all-gather.14.cloned.1.call-update
  134.5 0.0 reduce-scatter.2.cloned.1.call-start
  134.5 57.8 %all-gather.10.cloned.1.call-done = bf16[512,2048]{1,0:T(8,128)(2,1)} async-done(((bf16[128,2048]{1,0:T(8,128)(2,1)}), bf16[512,2048]{1,0:T(8,128)(2,1)}) %all-gather.10.cloned.1.call-update) | async-done | bytes 2097168 | tf_op jit(solution)/shard_map/all_gather | solution.py:107
  192.3 74.8 %all-gather.12.cloned.1.call-done = bf16[2048,1024]{1,0:T(8,128)(2,1)} async-done(((bf16[256,1024]{1,0:T(8,128)(2,1)}), bf16[2048,1024]{1,0:T(8,128)(2,1)}) %all-gather.12.cloned.1.call-update) | async-done | bytes 4194320 | tf_op jit(solution)/shard_map/all_gather | solution.py:101
  267.1 75.1 %all-gather.14.cloned.1.call-done = bf16[1024,2048]{1,0:T(8,128)(2,1)} async-done(((bf16[1024,256]{1,0:T(8,128)(2,1)}), bf16[1024,2048]{1,0:T(8,128)(2,1)}) %all-gather.14.cloned.1.call-update) | async-done | bytes 4194320 | tf_op jit(solution)/shard_map/all_gather | solution.py:102
  342.2 9.9 %convolution_convert_fusion = bf16[512,2048]{1,0:T(8,128)(2,1)} fusion(bf16[1024,2048]{1,0:T(8,128)(2,1)} %all-gather.14.cloned.1.call-done, bf16[512,2048]{1,0:T(8,128)(2,1)} %all-gather.10.cloned.1.call-done, bf16[2048,1024]{1,0:T(8,128)(2,1)} %all-gather.12.cloned.1.call-done), kind=kOutput, calls=%fused_computation.28 | convolution fusion | flops 4297588736 | bytes 12582912 | tf_op jit(solution)/shard_map/dot_general | solution.py:114
  352.1 0.0 reduce-scatter.2.cloned.1.call-update
  352.1 29.5 %reduce-scatter.2.cloned.1.call-done = bf16[128,2048]{1,0:T(8,128)(2,1)} async-done(((bf16[512,2048]{1,0:T(8,128)(2,1)}), bf16[128,2048]{1,0:T(8,128)(2,1)}) %reduce-scatter.2.cloned.1.call-update) | async-done | bytes 524304 | tf_op jit(solution)/shard_map/reduce_scatter | solution.py:113
  381.6 1.9 add_convert_fusion
  (31 shorter events, 0.3 us)
Async XLA Ops:
  6.5 55.9 %all-gather.6.cloned.1.call-start = ((), (), s32[]{:S(2)}) async-start(), calls=%async_computation.2 | async-start | bytes 2359296 | tf_op jit(solution)/shard_map/all_gather | solution.py:35
  8.4 104.7 %all-gather.8.cloned.1.call-start = ((), (), s32[]{:S(2)}) async-start(), calls=%async_computation.3 | async-start | bytes 2359296 | tf_op jit(solution)/shard_map/all_gather | solution.py:36
  10.2 182.1 %all-gather.10.cloned.1.call-start = ((), (), s32[]{:S(2)}) async-start(), calls=%async_computation.4 | async-start | bytes 2621440 | tf_op jit(solution)/shard_map/all_gather | solution.py:107
  113.2 6.1 %copy-start.2 = (f32[2]{0:T(128)S(1)}, f32[2]{0:T(128)}, u32[]{:S(2)}) copy-start(f32[2]{0:T(128)} %param.18) | copy-start | bytes 28
  113.2 6.6 %copy-start.3 = (f32[128]{0:T(128)S(1)}, f32[128]{0:T(128)}, u32[]{:S(2)}) copy-start(f32[128]{0:T(128)} %param.19) | copy-start | bytes 1540
  119.3 9.9 %copy-start = (bf16[128,2048]{1,0:T(8,128)(2,1)S(1)}, bf16[128,2048]{1,0:T(8,128)(2,1)}, u32[]{:S(2)}) copy-start(bf16[128,2048]{1,0:T(8,128)(2,1)} %param.14) | copy-start | bytes 1572868
  129.3 3.0 copy-start.1
  133.3 133.8 %all-gather.12.cloned.1.call-start = ((), (), s32[]{:S(2)}) async-start(), calls=%async_computation.5 | async-start | bytes 4718592 | tf_op jit(solution)/shard_map/all_gather | solution.py:101
  133.9 208.3 %all-gather.14.cloned.1.call-start = ((), (), s32[]{:S(2)}) async-start(), calls=%async_computation.6 | async-start | bytes 4718592 | tf_op jit(solution)/shard_map/all_gather | solution.py:102
  134.5 247.2 %reduce-scatter.2.cloned.1.call-start = ((), (), s32[]{:S(2)}) async-start(), calls=%async_computation.7 | async-start | bytes 2621440 | tf_op jit(solution)/shard_map/reduce_scatter | solution.py:113
Sparse Core Ops, SparseCore 0:
  9.4 53.0 all-gather.5
  64.5 48.5 all-gather.7
  133.4 58.8 all-gather.9
  194.3 72.7 all-gather.11
  269.0 73.1 all-gather.13
  352.3 29.3 reduce-scatter.1
where the time goes:
time: 391 us; the launch traced here: 390 us
  waiting for transfers between devices  340 us (87%)
  matrix products  15.6 us (4%)
  between operations  13.6 us (3%)
  blocking collectives  8.55 us (2%)
  local copies, waits for them, and re-layouts  7.41 us (2%)
  other arithmetic  4.49 us (1%)
    all_gather x1, waiting for transfers between devices, per_device(): lax.all_gather(down_weight, 'sp', axis=1, tiled=True)  75.1 us
    all_gather x1, waiting for transfers between devices, per_device(): lax.all_gather(up_weight, 'sp', axis=0, tiled=True)  74.8 us
    all_gather x1, waiting for transfers between devices, per_device(): lax.all_gather(normed, 'tp', axis=0, tiled=True)  57.8 us
    all_gather x1, waiting for transfers between devices, per_device(): key_piece = lax.all_gather(keys, 'sp', axis=0, tiled=True)  51.1 us
    all_gather x1, waiting for transfers between devices, per_device(): value_piece = lax.all_gather(values, 'sp', axis=0, tiled=True)  50.6 us
    reduce_scatter x1, waiting for transfers between devices, per_device(): lax.psum_scatter(jnp.dot(hidden, down_full, preferred_element_type=jnp.fl...  29.5 us
    dot_general x1, matrix products, per_device(): jnp.dot(hidden, down_full, preferred_element_type=jnp.float32)  9.93 us
    all_to_all x1, blocking collectives, per_device(): lax.all_to_all(attended, 'tp', split_axis=0, concat_axis=1, tiled=True)  8.55 us
  transfers between devices with their start and end apart: 6, of which 6 were waited for; matrix products, arithmetic and copies ran while one was open for 1% of the time, Pallas kernels for 0%

commit v1 on v0

--- a/solution.py
+++ b/solution.py
@@ -3,6 +3,7 @@
 import jax.numpy as jnp
 from jax import lax
 from jax.sharding import PartitionSpec as P
+from jax.lax import all_gather
 
 DQK = 64
 DV = 128
@@ -32,8 +33,9 @@
     zero_total = jnp.zeros((head_count, tok_rows), jnp.float32)
     zero_acc = jnp.zeros((head_count, tok_rows, DV), jnp.float32)
     start_state = (floor_max, zero_total, zero_acc, floor_max, zero_total, zero_acc)
-    key_piece = lax.all_gather(keys, "sp", axis=0, tiled=True)
-    value_piece = lax.all_gather(values, "sp", axis=0, tiled=True)
+    o_now = jnp.concatenate([keys, values], axis=1)
+    u1 = all_gather(o_now, "sp", axis=0, tiled=True)
+    key_piece, value_piece = jnp.split(u1, [keys.shape[1]], axis=1)
     piece_rows = key_piece.shape[0]
     block_width = math.gcd(piece_rows, 512)
 

time: 391 us -> 308 us (0.79)
  waiting for transfers between devices: 340 us -> 256 us
    all_gather x1, waiting for transfers between devices: 57.8 us -> 22.5 us  [per_device(): lax.all_gather(normed, 'tp', axis=0, tiled=True)]
    all_gather x2 -> x1, waiting for transfers between devices: 102 us -> 75.8 us  [per_device(): u1 = all_gather(o_now, 'sp', axis=0, tiled=True)]
    all_gather x1, waiting for transfers between devices: 75.1 us -> 51.6 us  [per_device(): lax.all_gather(down_weight, 'sp', axis=1, tiled=True)]
    split x0 -> x1, local copies, waits for them, and re-layouts: none -> 3.94 us  [per_device(): key_piece, value_piece = jnp.split(u1, [keys.shape[1]], axis=1)]
  transfers between devices with their start and end apart: 6 -> 5, of which waited for: 6 -> 5; matrix products, arithmetic and copies ran while one was open for 1% -> 5% of each run, Pallas kernels for 0% -> 0%
where the time goes in v1:
time: 308 us; the launch traced here: 307 us
  waiting for transfers between devices  256 us (83%)
  matrix products  15.6 us (5%)
  between operations  13.3 us (4%)
  blocking collectives  8.59 us (3%)
  local copies, waits for them, and re-layouts  8.09 us (3%)
  other arithmetic  5.32 us (2%)
    all_gather x1, waiting for transfers between devices, per_device(): u1 = all_gather(o_now, 'sp', axis=0, tiled=True)  75.8 us
    all_gather x1, waiting for transfers between devices, per_device(): lax.all_gather(up_weight, 'sp', axis=0, tiled=True)  73.1 us
    all_gather x1, waiting for transfers between devices, per_device(): lax.all_gather(down_weight, 'sp', axis=1, tiled=True)  51.6 us
    reduce_scatter x1, waiting for transfers between devices, per_device(): lax.psum_scatter(jnp.dot(hidden, down_full, preferred_element_type=jnp.fl...  31.3 us
    all_gather x1, waiting for transfers between devices, per_device(): lax.all_gather(normed, 'tp', axis=0, tiled=True)  22.5 us
    dot_general x1, matrix products, per_device(): jnp.dot(hidden, down_full, preferred_element_type=jnp.float32)  9.93 us
    all_to_all x1, blocking collectives, per_device(): lax.all_to_all(attended, 'tp', split_axis=0, concat_axis=1, tiled=True)  8.59 us
  transfers between devices with their start and end apart: 5, of which 5 were waited for; matrix products, arithmetic and copies ran while one was open for 5% of the time, Pallas kernels for 0%

profile of v1, /device:TPU:0, one launch (start us, length us, event | category | flops | bytes accessed | tf_op | source)
XLA Modules:
  0.0 307.5 jit_solution(1780233604180829738)
XLA Ops:
  6.5 0.0 copy-start.1
  6.5 0.0 all-gather.5.cloned.1.call-start
  6.5 1.1 copy.19
  7.7 1.1 copy.20
  8.8 0.8 pad_maximum_fusion
  9.6 0.0 all-gather.5.cloned.1.call-update
  9.6 0.0 all-gather.11.cloned.1.call-start
  9.7 0.7 all-gather.11.cloned.1.call-update
  10.4 0.0 all-gather.9.cloned.1.call-start
  10.4 0.7 all-gather.9.cloned.1.call-update
  11.1 0.0 all-gather.7.cloned.1.call-start
  11.2 0.0 copy-done.1
  11.2 0.1 copy.21
  11.4 75.8 %all-gather.5.cloned.1.call-done = bf16[4096,512]{0,1:T(8,128)(2,1)} async-done(((bf16[512,512]{0,1:T(8,128)(2,1)}), bf16[4096,512]{0,1:T(8,128)(2,1)}) %all-gather.5.cloned.1.call-update) | async-done | bytes 4194320 | tf_op jit(solution)/shard_map/all_gather | solution.py:37
  87.1 3.9 %fusion.22 = (bf16[4096,256]{0,1:T(8,128)(2,1)S(1)}, bf16[4096,256]{0,1:T(8,128)(2,1)}) fusion(bf16[4096,512]{0,1:T(8,128)(2,1)} %all-gather.5.cloned.1.call-done), kind=kLoop, calls=%fused_computation.48 | loop fusion | bytes 8388608 | tf_op jit(solution)/shard_map/split | solution.py:38
  91.2 0.0 copy-start.3
  91.2 0.0 copy-start.4
  91.2 5.1 %while.24 = (s32[]{:T(128)}, f32[2,512]{1,0:T(2,128)S(1)}, f32[2,512]{1,0:T(2,128)S(1)}, f32[2,512,128]{2,1,0:T(8,128)S(1)}, f32[2,512]{1,0:T(2,128)S(1)}, /*ind...) while((s32[]{:T(128)}, f32[2,512]{1,0:T(2,128)S(1)}, ...), condition=%wide.region_7.8_spmd.clone, body=%wide.region_0.7_spmd.clone.sunk | while | flops 410784768 | bytes 17707416 | solution.py:84
  91.3 4.6 %conditional.3 = ((f32[2,512]{1,0:T(2,128)S(1)}, f32[2,512]{1,0:T(2,128)S(1)}, f32[2,512,128]{2,1,0:T(8,128)S(1)}, f32[2,512]{1,0:T(2,128)S(1)}, f32[2,512]{1,0:T(2,128)S(1)}, /*index=5*/f32[2,512,128]{2,1,0:T(8,128)S(1)})) conditional(s32[]{:T(128)} %convert_element_type.94, (f32[2,512]{1,0:T(2,128)S(1)}, f32[2,512]{1,0:T(2,128)S(1)}, ...), branch_computations={%region_1.0_spmd, %region_2.6_spmd} | conditional | flops 410784768 | bytes 17705066 | solution.py:82
  91.3 1.0 constant_dynamic-slice_fusion.1
  92.3 0.2 broadcast_compare_fusion
  92.5 0.6 fusion.20
  93.2 0.3 fusion.3
  93.5 0.6 fusion.21
  94.1 0.3 fusion.5
  94.5 0.7 convolution_add_fusion
  95.2 0.7 convolution_add_fusion.1
  96.3 0.0 copy-done.3
  96.4 0.0 copy-start
  96.4 0.5 multiply_reduce_fusion.1
  96.9 0.0 copy-done.4
  96.9 0.2 fusion.18
  97.1 0.3 copy.23
  97.4 0.2 all_to_all.14
  97.6 8.6 %all_to_all.19 = bf16[4,128,256]{2,1,0:T(8,128)(2,1)S(1)} all-to-all(bf16[4,128,256]{2,1,0:T(8,128)(2,1)S(1)} %all_to_all.14), channel_id=1, replica_groups=mesh['sp'=8,'tp'=4] {'tp'}, dimensions={0} | all-to-all | bytes 524288 | tf_op jit(solution)/shard_map/all_to_all | solution.py:91
  106.2 0.2 copy.24
  106.3 0.0 copy-done
  106.3 0.0 copy-start.2
  106.4 3.0 multiply_reduce_fusion
  109.4 0.0 copy-done.2
  109.4 1.0 multiply_convert_fusion.1
  110.4 0.0 all-gather.7.cloned.1.call-update
  110.4 0.0 reduce-scatter.2.cloned.1.call-start
  110.4 51.6 %all-gather.11.cloned.1.call-done = bf16[1024,2048]{1,0:T(8,128)(2,1)} async-done(((bf16[1024,256]{1,0:T(8,128)(2,1)}), bf16[1024,2048]{1,0:T(8,128)(2,1)}) %all-gather.11.cloned.1.call-update) | async-done | bytes 4194320 | tf_op jit(solution)/shard_map/all_gather | solution.py:104
  162.0 73.1 %all-gather.9.cloned.1.call-done = bf16[2048,1024]{1,0:T(8,128)(2,1)} async-done(((bf16[256,1024]{1,0:T(8,128)(2,1)}), bf16[2048,1024]{1,0:T(8,128)(2,1)}) %all-gather.9.cloned.1.call-update) | async-done | bytes 4194320 | tf_op jit(solution)/shard_map/all_gather | solution.py:103
  235.2 22.5 %all-gather.7.cloned.1.call-done = bf16[512,2048]{1,0:T(8,128)(2,1)} async-done(((bf16[128,2048]{1,0:T(8,128)(2,1)}), bf16[512,2048]{1,0:T(8,128)(2,1)}) %all-gather.7.cloned.1.call-update) | async-done | bytes 2097168 | tf_op jit(solution)/shard_map/all_gather | solution.py:109
  257.7 9.9 %convolution_convert_fusion = bf16[512,2048]{1,0:T(8,128)(2,1)} fusion(bf16[1024,2048]{1,0:T(8,128)(2,1)} %all-gather.11.cloned.1.call-done, bf16[512,2048]{1,0:T(8,128)(2,1)} %all-gather.7.cloned.1.call-done, bf16[2048,1024]{1,0:T(8,128)(2,1)} %all-gather.9.cloned.1.call-done), kind=kOutput, calls=%fused_computation.28 | convolution fusion | flops 4297588736 | bytes 12582912 | tf_op jit(solution)/shard_map/dot_general | solution.py:116
  267.6 0.0 reduce-scatter.2.cloned.1.call-update
  267.7 31.3 %reduce-scatter.2.cloned.1.call-done = bf16[128,2048]{1,0:T(8,128)(2,1)} async-done(((bf16[512,2048]{1,0:T(8,128)(2,1)}), bf16[128,2048]{1,0:T(8,128)(2,1)}) %reduce-scatter.2.cloned.1.call-update) | async-done | bytes 524304 | tf_op jit(solution)/shard_map/reduce_scatter | solution.py:115
  299.0 1.9 add_convert_fusion
  (32 shorter events, 0.3 us)
Async XLA Ops:
  6.5 4.6 %copy-start.1 = (bf16[512,256]{1,0:T(8,128)(2,1)S(1)}, bf16[512,256]{1,0:T(8,128)(2,1)}, u32[]{:S(2)}) copy-start(bf16[512,256]{1,0:T(8,128)(2,1)} %param.15) | copy-start | bytes 786436
  6.5 80.6 %all-gather.5.cloned.1.call-start = ((), (), s32[]{:S(2)}) async-start(), calls=%async_computation.2 | async-start | bytes 4718592 | tf_op jit(solution)/shard_map/all_gather | solution.py:37
  9.6 152.4 %all-gather.11.cloned.1.call-start = ((), (), s32[]{:S(2)}) async-start(), calls=%async_computation.5 | async-start | bytes 4718592 | tf_op jit(solution)/shard_map/all_gather | solution.py:104
  10.4 224.8 %all-gather.9.cloned.1.call-start = ((), (), s32[]{:S(2)}) async-start(), calls=%async_computation.4 | async-start | bytes 4718592 | tf_op jit(solution)/shard_map/all_gather | solution.py:103
  11.1 246.6 %all-gather.7.cloned.1.call-start = ((), (), s32[]{:S(2)}) async-start(), calls=%async_computation.3 | async-start | bytes 2621440 | tf_op jit(solution)/shard_map/all_gather | solution.py:109
  91.2 5.1 %copy-start.3 = (f32[2]{0:T(128)S(1)}, f32[2]{0:T(128)}, u32[]{:S(2)}) copy-start(f32[2]{0:T(128)} %param.18) | copy-start | bytes 28
  91.2 5.7 %copy-start.4 = (f32[128]{0:T(128)S(1)}, f32[128]{0:T(128)}, u32[]{:S(2)}) copy-start(f32[128]{0:T(128)} %param.19) | copy-start | bytes 1540
  96.4 10.0 %copy-start = (bf16[128,2048]{1,0:T(8,128)(2,1)S(1)}, bf16[128,2048]{1,0:T(8,128)(2,1)}, u32[]{:S(2)}) copy-start(bf16[128,2048]{1,0:T(8,128)(2,1)} %param.14) | copy-start | bytes 1572868
  106.3 3.1 copy-start.2
  110.4 188.6 %reduce-scatter.2.cloned.1.call-start = ((), (), s32[]{:S(2)}) async-start(), calls=%async_computation.6 | async-start | bytes 2621440 | tf_op jit(solution)/shard_map/reduce_scatter | solution.py:115
Sparse Core Ops, SparseCore 0:
  9.8 77.3 all-gather.4
  89.2 72.8 all-gather.10
  164.2 70.9 all-gather.8
  236.6 21.0 all-gather.6
  267.8 31.1 reduce-scatter.1
